TPU v7x, 32 devices: a whole 2x2x4 slice. The times are simulated.
32 devices in a mesh: sp: 8 (over z, x), tp: 4 (over y, core).
Axes of the slice: x: 2, y: 2, z: 4, core: 2. Of those that a mesh axis runs over, the one named last changes fastest.
Arguments:
- q_first: bfloat16 [1536, 512], P('sp', 'tp'), may hold values from -6 to 6
- k_first: bfloat16 [1536, 512], P('sp', 'tp'), may hold values from -6 to 6
- q_second: bfloat16 [1536, 512], P('sp', 'tp'), may hold values from -6 to 6
- k_second: bfloat16 [1536, 512], P('sp', 'tp'), may hold values from -6 to 6
- values: bfloat16 [1536, 1024], P('sp', 'tp'), may hold values from -6 to 6
- lambdas: float32 [8], P('tp'), may hold values from 0.3 to 0.8
- head_gain: float32 [128], replicated, may hold values from 0.1 to 1.9
- out_weight: bfloat16 [1024, 2048], P('tp'), may hold values from -0.1875 to 0.1875
- residual_in: bfloat16 [1536, 2048], P('sp'), may hold values from -6 to 6
- mix_gain: float32 [2048], replicated, may hold values from 0.1 to 1.9
- gate_weight: bfloat16 [2048, 5632], P('sp', 'tp'), may hold values from -0.125 to 0.125
- up_weight: bfloat16 [2048, 5632], P('sp', 'tp'), may hold values from -0.125 to 0.125
- gate_taps: float32 [3, 5632], P(None, 'tp'), may hold values from -3.5 to 3.5
- up_taps: float32 [3, 5632], P(None, 'tp'), may hold values from -3.5 to 3.5
- down_weight: bfloat16 [5632, 2048], P('tp'), may hold values from -0.078125 to 0.078125
Outputs:
- mixed: bfloat16 [1536, 2048], P(('sp', 'tp'))
All inputs are finite; a program needn't handle non-finite values.
Results may differ from a plain program's by a relative error of at most 0.017.
Values may be sent and summed in bfloat16 or wider, within the bound.
A program may use at most 128 MiB of HBM per device.

v0:
```python
import jax
import jax.numpy as jnp
from jax import lax
from jax.sharding import PartitionSpec as P

norm_eps = 1e-06
far_below = -1e30


def passed_along(value, axis, steps):
    count = lax.axis_size(axis)
    initial, last = (max(0, -steps), min(count, count - steps))
    return lax.ppermute(value, axis, [(source, source + steps) for source in range(initial, last)])


def block_span(count, limit):
    return max((width for width in range(1, min(count, limit) + 1) if count % width == 0))


def update(peaks, totals, accum, scores, vals, visible):
    masked = jnp.where(visible, scores, far_below)
    new_peaks = jnp.maximum(peaks, jnp.max(masked, axis=-1))
    fade = jnp.exp(peaks - new_peaks)
    weights = jnp.where(visible, jnp.exp(masked - new_peaks[..., None]), 0.0)
    totals = totals * fade + jnp.sum(weights, axis=-1)
    accum = accum * fade.T[..., None] + jnp.einsum(
        "hqk,khv->qhv", weights.astype(jnp.bfloat16), vals, preferred_element_type=jnp.float32
    )
    return (new_peaks, totals, accum)


def rms_scale(field, gain):
    return field * lax.rsqrt(jnp.mean(field * field, axis=-1, keepdims=True) + norm_eps) * gain


def shards(
    q_first,
    k_first,
    q_second,
    k_second,
    values,
    lambdas,
    head_gain,
    out_weight,
    residual_in,
    mix_gain,
    gate_weight,
    up_weight,
    gate_taps,
    up_taps,
    down_weight,
):
    tok_rows = q_first.shape[0]
    head_count = lambdas.shape[0]
    head_dim = q_first.shape[1] // head_count
    value_dim = values.shape[1] // head_count
    part_rows = tok_rows // lax.axis_size("tp")
    tp_rank = lax.axis_index("tp")
    scale = head_dim ** (-0.5)
    query_pos = lax.axis_index("sp") * tok_rows + jnp.arange(tok_rows, dtype=jnp.int32)
    query_a = q_first.reshape(tok_rows, head_count, head_dim)
    query_b = q_second.reshape(tok_rows, head_count, head_dim)
    peaks_start = jnp.full((head_count, tok_rows), far_below, jnp.float32)
    totals_start = jnp.zeros((head_count, tok_rows), jnp.float32)
    accum_start = jnp.zeros((tok_rows, head_count, value_dim), jnp.float32)
    start = jnp.int32(0)
    keys_a = lax.all_gather(k_first, "sp", axis=0, tiled=True)
    keys_b = lax.all_gather(k_second, "sp", axis=0, tiled=True)
    vals = lax.all_gather(values, "sp", axis=0, tiled=True)
    count = keys_a.shape[0]
    span = block_span(count, 2048)

    def step(index, inner):
        peaks_a, totals_a, accum_a, peaks_b, totals_b, accum_b = inner
        offset = index * span
        block_a = lax.dynamic_slice_in_dim(keys_a, offset, span, 0).reshape(
            span, head_count, head_dim
        )
        block_b = lax.dynamic_slice_in_dim(keys_b, offset, span, 0).reshape(
            span, head_count, head_dim
        )
        block_v = lax.dynamic_slice_in_dim(vals, offset, span, 0).reshape(
            span, head_count, value_dim
        )
        key_pos = start + offset + jnp.arange(span, dtype=jnp.int32)
        visible = (key_pos[None, :] <= query_pos[:, None])[None]
        scores_a = (
            jnp.einsum("qhd,khd->hqk", query_a, block_a, preferred_element_type=jnp.float32) * scale
        )
        scores_b = (
            jnp.einsum("qhd,khd->hqk", query_b, block_b, preferred_element_type=jnp.float32) * scale
        )
        peaks_a, totals_a, accum_a = update(peaks_a, totals_a, accum_a, scores_a, block_v, visible)
        peaks_b, totals_b, accum_b = update(peaks_b, totals_b, accum_b, scores_b, block_v, visible)
        return (peaks_a, totals_a, accum_a, peaks_b, totals_b, accum_b)

    carry = lax.fori_loop(
        0,
        count // span,
        step,
        (peaks_start, totals_start, accum_start, peaks_start, totals_start, accum_start),
    )
    first = carry[2] / carry[1].T[..., None]
    second = carry[5] / carry[4].T[..., None]
    diff_heads = first - lambdas[None, :, None] * second
    head_out = (
        rms_scale(diff_heads, head_gain)
        .astype(jnp.bfloat16)
        .reshape(tok_rows, head_count * value_dim)
    )
    attended = lax.psum_scatter(
        jnp.dot(head_out, out_weight, preferred_element_type=jnp.float32).astype(jnp.bfloat16),
        "tp",
        scatter_dimension=0,
        tiled=True,
    ).astype(jnp.float32)
    own_rows = lax.dynamic_slice_in_dim(residual_in, tp_rank * part_rows, part_rows, 0)
    stream_rows = own_rows.astype(jnp.float32) + attended
    normed_part = rms_scale(stream_rows, mix_gain).astype(jnp.bfloat16)
    ffn_in = lax.all_gather(normed_part, "tp", axis=0, tiled=True)
    gate_pre = jnp.dot(
        ffn_in,
        lax.all_gather(gate_weight, "sp", axis=0, tiled=True),
        preferred_element_type=jnp.float32,
    )
    up_pre = jnp.dot(
        ffn_in,
        lax.all_gather(up_weight, "sp", axis=0, tiled=True),
        preferred_element_type=jnp.float32,
    )
    projected = jnp.stack((gate_pre.astype(jnp.bfloat16), up_pre.astype(jnp.bfloat16)))
    tap_count = gate_taps.shape[0]
    edge = passed_along(projected[:, tok_rows - (tap_count - 1) :], "sp", 1)
    padded = jnp.concatenate((edge, projected), axis=1).astype(jnp.float32)
    taps = jnp.stack((gate_taps, up_taps))
    convolved = taps[:, 0][:, None, :] * padded[:, 0:tok_rows]
    for offset in range(1, tap_count):
        convolved = convolved + taps[:, offset][:, None, :] * padded[:, offset : offset + tok_rows]
    hidden = (jax.nn.silu(convolved[0]) * convolved[1]).astype(jnp.bfloat16)
    down_rows = lax.psum_scatter(
        jnp.dot(hidden, down_weight, preferred_element_type=jnp.float32).astype(jnp.bfloat16),
        "tp",
        scatter_dimension=0,
        tiled=True,
    ).astype(jnp.float32)
    return (stream_rows + down_rows).astype(jnp.bfloat16)


def solution(mesh):
    in_specs = (
        P("sp", "tp"),
        P("sp", "tp"),
        P("sp", "tp"),
        P("sp", "tp"),
        P("sp", "tp"),
        P("tp"),
        P(),
        P("tp", None),
        P("sp", None),
        P(),
        P("sp", "tp"),
        P("sp", "tp"),
        P(None, "tp"),
        P(None, "tp"),
        P("tp", None),
    )
    out_specs = P(("sp", "tp"), None)
    return jax.shard_map(shards, mesh=mesh, in_specs=in_specs, out_specs=out_specs, check_vma=False)
```

profile of v0, /device:TPU:19, one launch (start us, length us, event | category | flops | bytes accessed | tf_op | source)
XLA Modules:
  0.0 359.3 jit_solution(8689654053603012556)
XLA Ops:
  7.4 0.0 copy-start
  7.4 0.0 reduce-scatter.3.cloned.1.call-start
  7.4 0.0 copy-start.7
  7.4 0.9 iota_compare_fusion
  8.3 23.3 %all_gather.18 = bf16[1536,128]{1,0:T(8,128)(2,1)S(1)} all-gather(bf16[192,128]{1,0:T(8,128)(2,1)} %param.16), channel_id=1, replica_groups=mesh['sp'=8,'tp'=4] {'sp'}, dimensions={0}, use_global_device_ids=true | all-gather | bytes 442368 | tf_op jit(solution)/shard_map/all_gather | solution.py:67
  31.6 0.9 copy.29
  32.5 0.9 copy.28
  33.4 1.8 fusion.55
  35.3 0.0 copy-done.7
  35.3 26.6 %all_gather.20 = bf16[1536,128]{1,0:T(8,128)(2,1)} all-gather(bf16[192,128]{1,0:T(8,128)(2,1)S(1)} %copy-done.7), channel_id=1, replica_groups=mesh['sp'=8,'tp'=4] {'sp'}, dimensions={0}, use_global_device_ids=true | all-gather | bytes 442368 | tf_op jit(solution)/shard_map/all_gather | solution.py:68
  61.9 1.9 copy.33
  63.8 0.9 copy.32
  64.7 0.0 copy-start.6
  64.7 3.2 fusion.54
  67.9 0.0 copy-done.6
  67.9 29.8 %all_gather.19 = bf16[1536,256]{1,0:T(8,128)(2,1)} all-gather(bf16[192,256]{1,0:T(8,128)(2,1)S(1)} %copy-done.6), channel_id=1, replica_groups=mesh['sp'=8,'tp'=4] {'sp'}, dimensions={0}, use_global_device_ids=true | all-gather | bytes 884736 | tf_op jit(solution)/shard_map/all_gather | solution.py:69
  97.7 2.3 copy.30
  100.0 0.0 copy-start.1
  100.0 0.0 copy-start.2
  100.0 3.0 fusion.6
  103.1 0.0 copy-done.1
  103.1 0.0 copy-done.2
  103.1 0.0 copy-done.4
  103.1 0.0 copy-done.12
  103.1 0.7 fusion.41
  103.9 0.0 copy-start.11
  103.9 0.8 multiply_reduce_fusion.1
  104.7 0.0 copy-start.8
  104.7 0.0 copy-start.9
  104.7 0.0 copy-start.5
  104.7 0.0 copy-done
  104.8 0.0 copy-done.11
  104.8 0.0 copy-start.10
  104.8 1.3 convolution_convert_fusion.3
  106.1 0.0 reduce-scatter.3.cloned.1.call-update
  106.1 0.0 all-gather.3.cloned.1.call-start
  106.2 0.5 all-gather.3.cloned.1.call-update
  106.7 0.0 all-gather.5.cloned.1.call-start
  106.7 0.5 all-gather.5.cloned.1.call-update
  107.3 0.0 reduce-scatter.5.cloned.1.call-start
  107.3 0.0 copy-done.8
  107.3 0.0 copy-done.9
  107.4 41.8 %reduce-scatter.3.cloned.1.call-done = bf16[48,2048]{1,0:T(8,128)(2,1)} async-done(((bf16[192,2048]{1,0:T(8,128)(2,1)}), bf16[48,2048]{1,0:T(8,128)(2,1)}) %reduce-scatter.3.cloned.1.call-update) | async-done | bytes 196624 | tf_op jit(solution)/shard_map/reduce_scatter | solution.py:111
  149.2 0.0 copy-done.5
  149.2 1.1 multiply_reduce_fusion
  150.3 0.0 copy-done.10
  150.3 1.0 multiply_convert_fusion
  151.4 8.7 %all_gather.21 = bf16[192,2048]{1,0:T(8,128)(2,1)S(1)} all-gather(bf16[48,2048]{1,0:T(8,128)(2,1)S(1)} %multiply_convert_fusion), channel_id=1, replica_groups=mesh['sp'=8,'tp'=4] {'tp'}, dimensions={0}, use_global_device_ids=true | all-gather | bytes 983040 | tf_op jit(solution)/shard_map/all_gather | solution.py:120
  160.1 57.8 %all-gather.3.cloned.1.call-done = bf16[2048,1408]{1,0:T(8,128)(2,1)} async-done(((bf16[256,1408]{1,0:T(8,128)(2,1)}), bf16[2048,1408]{1,0:T(8,128)(2,1)}) %all-gather.3.cloned.1.call-update) | async-done | bytes 5767184 | tf_op jit(solution)/shard_map/all_gather | solution.py:123
  217.9 4.0 %fusion.2 = bf16[1,192,1408]{2,1,0:T(8,128)(2,1)S(1)} fusion(bf16[192,2048]{1,0:T(8,128)(2,1)S(1)} %all_gather.21, bf16[2048,1408]{1,0:T(8,128)(2,1)} %all-gather.3.cloned.1.call-done), kind=kOutput, calls=%fused_computation.8 | convolution fusion | flops 1107566592 | bytes 7094272 | tf_op jit(solution)/shard_map/dot_general | solution.py:121
  221.9 88.3 %all-gather.5.cloned.1.call-done = bf16[2048,1408]{1,0:T(8,128)(2,1)} async-done(((bf16[256,1408]{1,0:T(8,128)(2,1)}), bf16[2048,1408]{1,0:T(8,128)(2,1)}) %all-gather.5.cloned.1.call-update) | async-done | bytes 5767184 | tf_op jit(solution)/shard_map/all_gather | solution.py:128
  310.3 4.0 %fusion.3 = bf16[1,192,1408]{2,1,0:T(8,128)(2,1)S(1)} fusion(bf16[192,2048]{1,0:T(8,128)(2,1)S(1)} %all_gather.21, bf16[2048,1408]{1,0:T(8,128)(2,1)} %all-gather.5.cloned.1.call-done), kind=kOutput, calls=%fused_computation.9 | convolution fusion | flops 1107566592 | bytes 7094272 | tf_op jit(solution)/shard_map/dot_general | solution.py:126
  314.3 4.2 %collective-permute-start = (bf16[2,2,1408]{2,1,0:T(2,128)(2,1)S(1)}, bf16[2,2,1408]{2,1,0:T(2,128)(2,1)S(1)}, u32[]{:S(2)}, u32[]{:S(2)}) collective-permute-start(bf16[2,2,1408]{2,1,0:T(2,128)(2,1)S(1)} %pad_maximum_fusion.2), channel_id=1, source_target_pairs={{0,4},{4,8},{8,12},{12,16},{16,20},{20,24},{24,28},{1,5},{5,9},{9,... | collective-permute-start | bytes 33800 | tf_op jit(solution)/shard_map/ppermute | solution.py:13
  318.6 0.8 collective-permute-done
  319.3 0.2 maximum_convert_fusion
  319.6 0.0 slice-start.1
  319.6 0.6 fusion.4
  320.2 1.3 slice-done
  321.5 0.6 slice-done.1
  322.1 2.4 convolution_convert_fusion
  324.4 0.0 reduce-scatter.5.cloned.1.call-update
  324.5 25.7 %reduce-scatter.5.cloned.1.call-done = bf16[48,2048]{1,0:T(8,128)(2,1)} async-done(((bf16[192,2048]{1,0:T(8,128)(2,1)}), bf16[48,2048]{1,0:T(8,128)(2,1)}) %reduce-scatter.5.cloned.1.call-update) | async-done | bytes 196624 | tf_op jit(solution)/shard_map/reduce_scatter | solution.py:140
  350.2 0.0 copy-done.3
  350.2 1.7 add_convert_fusion
  (15 shorter events, 0.1 us)
Async XLA Ops:
  7.4 97.4 %copy-start = (bf16[256,2048]{1,0:T(8,128)(2,1)S(1)}, bf16[256,2048]{1,0:T(8,128)(2,1)}, u32[]{:S(2)}) copy-start(bf16[256,2048]{1,0:T(8,128)(2,1)} %param.22) | copy-start | bytes 3145732
  7.4 141.8 %reduce-scatter.3.cloned.1.call-start = ((), (), s32[]{:S(2)}) async-start(), calls=%async_computation.2 | async-start | bytes 983040 | tf_op jit(solution)/shard_map/reduce_scatter | solution.py:111
  7.4 27.9 %copy-start.7 = (bf16[192,128]{1,0:T(8,128)(2,1)S(1)}, bf16[192,128]{1,0:T(8,128)(2,1)}, u32[]{:S(2)}) copy-start(bf16[192,128]{1,0:T(8,128)(2,1)} %param.18) | copy-start | bytes 147460
  64.7 3.2 copy-start.6
  100.0 3.1 copy-start.1
  100.0 3.1 copy-start.2
  100.0 3.1 copy-start.4
  100.0 3.1 copy-start.12
  103.9 0.9 copy-start.11
  104.7 2.6 copy-start.8
  104.7 2.6 copy-start.9
  104.7 44.5 %copy-start.5 = (bf16[192,2048]{1,0:T(8,128)(2,1)S(1)}, bf16[192,2048]{1,0:T(8,128)(2,1)}, u32[]{:S(2)}) copy-start(bf16[192,2048]{1,0:T(8,128)(2,1)} %param.23) | copy-start | bytes 2359300
  104.8 45.6 %copy-start.10 = (f32[2048]{0:T(1024)S(1)}, f32[2048]{0:T(1024)}, u32[]{:S(2)}) copy-start(f32[2048]{0:T(1024)} %param.24) | copy-start | bytes 24580
  106.1 111.8 %all-gather.3.cloned.1.call-start = ((), (), s32[]{:S(2)}) async-start(), calls=%async_computation.3 | async-start | bytes 6488064 | tf_op jit(solution)/shard_map/all_gather | solution.py:123
  106.7 203.6 %all-gather.5.cloned.1.call-start = ((), (), s32[]{:S(2)}) async-start(), calls=%async_computation.4 | async-start | bytes 6488064 | tf_op jit(solution)/shard_map/all_gather | solution.py:128
  107.3 242.9 %reduce-scatter.5.cloned.1.call-start = ((), (), s32[]{:S(2)}) async-start(), calls=%async_computation.5 | async-start | bytes 983040 | tf_op jit(solution)/shard_map/reduce_scatter | solution.py:140
  314.3 5.0 %collective-permute-start = (bf16[2,2,1408]{2,1,0:T(2,128)(2,1)S(1)}, bf16[2,2,1408]{2,1,0:T(2,128)(2,1)S(1)}, u32[]{:S(2)}, u32[]{:S(2)}) collective-permute-start(bf16[2,2,1408]{2,1,0:T(2,128)(2,1)S(1)} %pad_maximum_fusion.2), channel_id=1, source_target_pairs={{0,4},{4,8},{8,12},{12,16},{16,20},{20,24},{24,28},{1,5},{5,9},{9,... | collective-permute-start | bytes 33800 | tf_op jit(solution)/shard_map/ppermute | solution.py:13
  319.3 2.2 slice-start
  319.6 2.5 slice-start.1
  322.1 28.1 %copy-start.3 = (bf16[48,2048]{1,0:T(8,128)(2,1)S(1)}, bf16[48,2048]{1,0:T(8,128)(2,1)}, u32[]{:S(2)}) copy-start(bf16[48,2048]{1,0:T(8,128)(2,1)} %reduce-scatter.3.cloned.1.call-done) | copy-start | bytes 589828
Sparse Core Ops, SparseCore 0:
  106.2 42.9 reduce-scatter.2
  324.6 25.5 reduce-scatter.4
Sparse Core Ops, SparseCore 1:
  108.8 109.1 all-gather.2
  220.0 90.3 all-gather.4
where the time goes:
time: 362 us; the launch traced here: 359 us
  waiting for transfers between devices  216 us (60%)
  blocking collectives  88.4 us (24%)
  matrix products  18.3 us (5%)
  between operations  15.1 us (4%)
  local copies, waits for them, and re-layouts  8.85 us (2%)
  other arithmetic  8.77 us (2%)
  starting transfers between devices  4.33 us (1%)
    all_gather x1, waiting for transfers between devices, shards(): lax.all_gather(up_weight, 'sp', axis=0, tiled=True)  88.3 us
    all_gather x1, waiting for transfers between devices, shards(): lax.all_gather(gate_weight, 'sp', axis=0, tiled=True)  57.8 us
    reduce_scatter x1, waiting for transfers between devices, shards(): lax.psum_scatter(jnp.dot(head_out, out_weight, preferred_element_type=jnp...  41.8 us
    all_gather x1, blocking collectives, shards(): vals = lax.all_gather(values, 'sp', axis=0, tiled=True)  29.8 us
    all_gather x1, blocking collectives, shards(): keys_b = lax.all_gather(k_second, 'sp', axis=0, tiled=True)  26.6 us
    reduce_scatter x1, waiting for transfers between devices, shards(): lax.psum_scatter(jnp.dot(hidden, down_weight, preferred_element_type=jnp....  25.7 us
    all_gather x1, blocking collectives, shards(): keys_a = lax.all_gather(k_first, 'sp', axis=0, tiled=True)  23.3 us
    all_gather x1, blocking collectives, shards(): ffn_in = lax.all_gather(normed_part, 'tp', axis=0, tiled=True)  8.71 us
  transfers between devices with their start and end apart: 5, of which 5 were waited for; matrix products, arithmetic and copies ran while one was open for 2% of the time, Pallas kernels for 0%

commit v1 on v0

v1 whole, which is shorter than its diff:
```python
import functools

import jax
import jax.numpy as jnp
from jax import lax
from jax.experimental import pallas as pl
from jax.experimental.pallas import tpu as pltpu
from jax.sharding import PartitionSpec as P

norm_eps = 1e-06
far_below = -1e30
halo = 16
lanes = 2
f32 = jnp.float32
bf16 = jnp.bfloat16


def rms_scale(field, gain):
    return field * lax.rsqrt(jnp.mean(field * field, axis=-1, keepdims=True) + norm_eps) * gain


def layer(
    sp_count,
    tp_count,
    q_a,
    k_a,
    q_b,
    k_b,
    vals,
    lambdas,
    head_gain,
    out_weight,
    residual,
    mix_gain,
    gate_weight,
    up_weight,
    gate_taps,
    up_taps,
    down_weight,
    out,
    kv,
    w,
    down,
    out_w,
    res,
    heads,
    part_out,
    part_in,
    stream,
    ffn,
    acc,
    hidden,
    last_out,
    last_in,
    local,
    kvz_send,
    kvz_recv,
    kvx_send,
    kvx_recv,
    wz_send,
    wz_recv,
    wx_send,
    wx_recv,
    rs_send,
    rs_recv,
    ag_send,
    ag_recv,
    halo_send,
    halo_recv,
    last_send,
    last_recv,
):
    s = lax.axis_index("sp")
    t = lax.axis_index("tp")
    x = lax.rem(s, lanes)
    z = s // lanes
    lines = sp_count // lanes
    mate = z * lanes + (1 - x)
    rows = q_a.shape[0]
    key_width = q_a.shape[1]
    value_width = vals.shape[1]
    head_count = lambdas.shape[0]
    head_dim = key_width // head_count
    value_dim = value_width // head_count
    part = rows // tp_count
    width = out.shape[1]
    w_rows = gate_weight.shape[0]
    ff = gate_weight.shape[1]
    taps = gate_taps.shape[0]

    def remote(src, dst, send, recv, sp, tp):
        return pltpu.make_async_remote_copy(
            src_ref=src,
            dst_ref=dst,
            send_sem=send,
            recv_sem=recv,
            device_id=(sp, tp),
            device_id_type=pl.DeviceIdType.MESH,
        )

    def kv_block(block):
        return kv.at[pl.ds(pl.multiple_of(block * rows, 16), rows)]

    def w_block(c, block):
        return w.at[c, pl.ds(pl.multiple_of(block * w_rows, 16), w_rows)]

    own = pl.ds(pl.multiple_of(s * rows, 16), rows)
    kv_loads = (
        pltpu.make_async_copy(k_a, kv.at[own, pl.ds(0, key_width)], local.at[0]),
        pltpu.make_async_copy(k_b, kv.at[own, pl.ds(key_width, key_width)], local.at[1]),
        pltpu.make_async_copy(vals, kv.at[own, pl.ds(2 * key_width, value_width)], local.at[2]),
    )
    w_loads = (
        pltpu.make_async_copy(gate_weight, w_block(0, s), local.at[3]),
        pltpu.make_async_copy(up_weight, w_block(1, s), local.at[4]),
    )
    out_load = pltpu.make_async_copy(out_weight, out_w, local.at[5])
    res_load = pltpu.make_async_copy(
        residual.at[pl.ds(pl.multiple_of(t * part, 16), part)], res, local.at[6]
    )
    down_load = pltpu.make_async_copy(down_weight, down, local.at[7])
    for load in kv_loads + w_loads + (out_load, res_load, down_load):
        load.start()

    barrier = pltpu.get_barrier_semaphore()

    @pl.loop(1, sp_count)
    def _(i):
        pl.semaphore_signal(
            barrier,
            inc=1,
            device_id=(lax.rem(s + i, sp_count), t),
            device_id_type=pl.DeviceIdType.MESH,
        )

    @pl.loop(1, tp_count)
    def _(i):
        pl.semaphore_signal(
            barrier,
            inc=1,
            device_id=(s, lax.rem(t + i, tp_count)),
            device_id_type=pl.DeviceIdType.MESH,
        )

    pl.semaphore_wait(barrier, sp_count + tp_count - 2)

    def kvz(line, to, index):
        block = kv_block(line * lanes + x)
        return remote(block, block, kvz_send.at[index], kvz_recv.at[line], to * lanes + x, t)

    def kvx(line, lane):
        block = kv_block(line * lanes + lane)
        return remote(block, block, kvx_send.at[line], kvx_recv.at[line], mate, t)

    def wz(c, line, to, index):
        block = w_block(c, line * lanes + x)
        return remote(block, block, wz_send.at[c, index], wz_recv.at[c, line], to * lanes + x, t)

    def wx(c, line, lane):
        block = w_block(c, line * lanes + lane)
        return remote(block, block, wx_send.at[c, line], wx_recv.at[c, line], mate, t)

    for load in kv_loads:
        load.wait()

    @pl.loop(z + 1, lines)
    def _(to):
        kvz(z, to, to).start()

    kvx(z, x).start()
    for load in w_loads:
        load.wait()

    @pl.loop(1, lines)
    def _(i):
        to = lax.rem(z + lines - i, lines)
        for c in range(2):
            wz(c, z, to, to).start()

    @pl.loop(0, z)
    def _(i):
        line = z - 1 - i
        kvz(line, mate // lanes, line).wait_recv()
        kvx(line, x).start()

    for c in range(2):
        wx(c, z, x).start()

    scale = head_dim**-0.5
    column = lax.broadcasted_iota(jnp.int32, (rows, key_width), 1) // head_dim
    queries = [
        jnp.where(column == h, q[...], jnp.zeros((), bf16))
        for q in (q_a, q_b)
        for h in range(head_count)
    ]
    span = lanes * rows
    query_pos = s * rows + lax.broadcasted_iota(jnp.int32, (rows, span), 0)
    key_step = lax.broadcasted_iota(jnp.int32, (rows, span), 1)

    def attend(i, state):
        line = z - i
        kvx(line, 1 - x).wait_recv()
        keys_at = pl.ds(pl.multiple_of(line * span, 16), span)
        visible = line * span + key_step <= query_pos
        following = []
        for m in range(2):
            keys = kv[keys_at, pl.ds(m * key_width, key_width)]
            for h in range(head_count):
                peak, total, sums = state[m * head_count + h]
                value = kv[keys_at, pl.ds(2 * key_width + h * value_dim, value_dim)]
                scores = (
                    lax.dot_general(
                        queries[m * head_count + h],
                        keys,
                        (((1,), (1,)), ((), ())),
                        preferred_element_type=f32,
                    )
                    * scale
                )
                scores = jnp.where(visible, scores, far_below)
                new_peak = jnp.maximum(peak, jnp.max(scores, axis=-1, keepdims=True))
                fade = jnp.exp(peak - new_peak)
                expo = jnp.exp(scores - new_peak)
                total = total * fade + jnp.sum(expo, axis=-1, keepdims=True)
                sums = sums * fade + jnp.dot(expo.astype(bf16), value, preferred_element_type=f32)
                following.append((new_peak, total, sums))
        return tuple(following)

    start = tuple(
        (
            jnp.full((rows, 1), far_below, f32),
            jnp.zeros((rows, 1), f32),
            jnp.zeros((rows, value_dim), f32),
        )
        for _ in range(2 * head_count)
    )
    state = lax.fori_loop(0, z + 1, attend, start)
    for h in range(head_count):
        _, total_a, sums_a = state[h]
        _, total_b, sums_b = state[head_count + h]
        diff = sums_a / total_a - lambdas[h] * (sums_b / total_b)
        heads[:, h * value_dim : (h + 1) * value_dim] = rms_scale(diff, head_gain[...]).astype(bf16)

    def forward(i):
        line = lax.rem(z + i, lines)
        for c in range(2):
            wz(c, line, mate // lanes, line).wait_recv()
            wx(c, line, x).start()

    early = min(2, lines - 1)
    if early > 0:
        forward(1)

    out_load.wait()
    res_load.wait()
    stream[...] = res[...].astype(f32)

    def part_copy(i):
        to = lax.rem(t + i, tp_count)
        return remote(part_out.at[to], part_in.at[t], rs_send.at[to], rs_recv.at[t], s, to)

    for i in range(1, tp_count + 1):
        to = lax.rem(t + i, tp_count)
        product = jnp.dot(
            heads[pl.ds(pl.multiple_of(to * part, 16), part), :],
            out_w[...],
            preferred_element_type=f32,
        )
        if i < tp_count:
            part_out[to] = product.astype(bf16)
            part_copy(i).start()
        else:
            stream[...] += product
    for i in range(1, tp_count):
        source = lax.rem(t + i, tp_count)
        remote(
            part_out.at[source], part_in.at[source], rs_send.at[source], rs_recv.at[source], s, source
        ).wait_recv()
        stream[...] += part_in[source].astype(f32)

    def ffn_rows(rank):
        return pl.ds(pl.multiple_of(halo + rank * part, 16), part)

    ffn[ffn_rows(t), :] = rms_scale(stream[...], mix_gain[...]).astype(bf16)

    def gather_copy(i, rank):
        to = lax.rem(t + i, tp_count)
        piece = ffn.at[ffn_rows(rank)]
        return remote(piece, piece, ag_send.at[to], ag_recv.at[rank], s, to)

    for i in range(1, tp_count):
        gather_copy(i, t).start()
    if early > 1:
        forward(2)
    for i in range(1, tp_count):
        gather_copy(i, lax.rem(t + i, tp_count)).wait_recv()

    halo_copy = remote(
        ffn.at[pl.ds(rows, halo)],
        ffn.at[pl.ds(0, halo)],
        halo_send,
        halo_recv,
        lax.rem(s + 1, sp_count),
        t,
    )

    @pl.when(s < sp_count - 1)
    def _():
        halo_copy.start()

    @pl.when(s == 0)
    def _():
        ffn[0:halo, :] = jnp.zeros((halo, width), bf16)

    @pl.when(s > 0)
    def _():
        halo_copy.wait_recv()

    acc[...] = jnp.zeros_like(acc)

    def project(first, count):
        at = pl.ds(pl.multiple_of(first, 128), count)
        for c in range(2):
            acc[c] += jnp.dot(ffn[:, at], w[c, at, :], preferred_element_type=f32)

    line_rows = lanes * w_rows
    paced = line_rows % 128 == 0

    def arrive(i):
        line = lax.rem(z + i, lines)
        for c in range(2):
            wx(c, line, 1 - x).wait_recv()
        if paced:
            project(line * line_rows, line_rows)

    if paced:
        for i in range(early + 1, lines):
            arrive(i - early - 1)
            forward(i)

        @pl.loop(max(lines - early - 1, 0), lines)
        def _(i):
            arrive(i)
    else:

        @pl.loop(early + 1, lines)
        def _(i):
            forward(i)

        @pl.loop(0, lines)
        def _(i):
            arrive(i)

        @pl.loop(0, width // 256)
        def _(i):
            project(i * 256, 256)

    @pl.loop(0, ff // 128)
    def _(i):
        at = pl.ds(pl.multiple_of(i * 128, 128), 128)
        made = []
        for c, tap in enumerate((gate_taps, up_taps)):
            total = None
            for k in range(taps):
                row = acc[c, pl.ds(halo - taps + 1 + k, rows), at].astype(bf16).astype(f32)
                term = tap[pl.ds(k, 1), at] * row
                total = term if total is None else total + term
            made.append(total)
        hidden[:, at] = (made[0] / (1 + jnp.exp(-made[0])) * made[1]).astype(bf16)

    down_load.wait()
    chunk = last_out.shape[3]

    def last_copy(i, n, rank_to, rank_from):
        return remote(
            last_out.at[rank_to, n],
            last_in.at[rank_from, n],
            last_send.at[rank_to, n],
            last_recv.at[rank_from, n],
            s,
            lax.rem(t + i, tp_count),
        )

    for n in range(width // chunk):
        product = jnp.dot(
            hidden[...], down[:, n * chunk : (n + 1) * chunk], preferred_element_type=f32
        ).astype(bf16)
        for r in range(tp_count):
            last_out[r, n] = product[r * part : (r + 1) * part]
        for i in range(1, tp_count):
            last_copy(i, n, lax.rem(t + i, tp_count), t).start()
    for n in range(width // chunk):
        at = slice(n * chunk, (n + 1) * chunk)
        total = stream[:, at] + last_out[t, n].astype(f32)
        for i in range(1, tp_count):
            source = lax.rem(t + i, tp_count)
            last_copy(i, n, source, source).wait_recv()
            total = total + last_in[source, n].astype(f32)
        out[:, at] = total.astype(bf16)

    @pl.loop(z + 1, lines)
    def _(to):
        kvz(z, to, to).wait_send()

    @pl.loop(0, z + 1)
    def _(line):
        kvx(line, x).wait_send()

    @pl.loop(1, lines)
    def _(i):
        to = lax.rem(z + i, lines)
        for c in range(2):
            wz(c, z, to, to).wait_send()

    @pl.loop(0, lines)
    def _(line):
        for c in range(2):
            wx(c, line, x).wait_send()

    for i in range(1, tp_count):
        part_copy(i).wait_send()
        gather_copy(i, t).wait_send()
        for n in range(width // chunk):
            last_copy(i, n, lax.rem(t + i, tp_count), t).wait_send()

    @pl.when(s < sp_count - 1)
    def _():
        halo_copy.wait_send()


def shards(sp_count, tp_count, *args):
    (q_a, _, _, _, vals, lambdas, head_gain, out_weight, residual, mix_gain, gate, _, _, _, down) = args
    rows = q_a.shape[0]
    width = residual.shape[1]
    w_rows, ff = gate.shape
    part = rows // tp_count
    lines = sp_count // lanes
    chunk = 512 if width % 512 == 0 else width
    args = list(args)
    args[6] = head_gain.reshape(1, -1)
    args[9] = mix_gain.reshape(1, -1)
    vmem = pl.BlockSpec(memory_space=pltpu.VMEM)
    hbm = pl.BlockSpec(memory_space=pl.ANY)
    smem = pl.BlockSpec(memory_space=pltpu.SMEM)
    dma = pltpu.SemaphoreType.DMA
    in_specs = [vmem, hbm, vmem, hbm, hbm, smem, vmem, hbm, hbm, vmem, hbm, hbm, vmem, vmem, hbm]
    return pl.pallas_call(
        functools.partial(layer, sp_count, tp_count),
        out_shape=jax.ShapeDtypeStruct((part, width), bf16),
        in_specs=in_specs,
        out_specs=vmem,
        scratch_shapes=[
            pltpu.VMEM((sp_count * rows, 2 * q_a.shape[1] + vals.shape[1]), bf16),
            pltpu.VMEM((2, sp_count * w_rows, ff), bf16),
            pltpu.VMEM(down.shape, bf16),
            pltpu.VMEM(out_weight.shape, bf16),
            pltpu.VMEM((part, width), bf16),
            pltpu.VMEM((rows, vals.shape[1]), bf16),
            pltpu.VMEM((tp_count, part, width), bf16),
            pltpu.VMEM((tp_count, part, width), bf16),
            pltpu.VMEM((part, width), f32),
            pltpu.VMEM((halo + rows, width), bf16),
            pltpu.VMEM((2, halo + rows, ff), f32),
            pltpu.VMEM((rows, ff), bf16),
            pltpu.VMEM((tp_count, width // chunk, part, chunk), bf16),
            pltpu.VMEM((tp_count, width // chunk, part, chunk), bf16),
            dma((8,)),
            dma((lines,)),
            dma((lines,)),
            dma((lines,)),
            dma((lines,)),
            dma((2, lines)),
            dma((2, lines)),
            dma((2, lines)),
            dma((2, lines)),
            dma((tp_count,)),
            dma((tp_count,)),
            dma((tp_count,)),
            dma((tp_count,)),
            dma(()),
            dma(()),
            dma((tp_count, width // chunk)),
            dma((tp_count, width // chunk)),
        ],
        compiler_params=pltpu.CompilerParams(
            collective_id=0, has_side_effects=True, vmem_limit_bytes=60 * 1024 * 1024
        ),
    )(*args)


def solution(mesh):
    in_specs = (
        P("sp", "tp"),
        P("sp", "tp"),
        P("sp", "tp"),
        P("sp", "tp"),
        P("sp", "tp"),
        P("tp"),
        P(),
        P("tp", None),
        P("sp", None),
        P(),
        P("sp", "tp"),
        P("sp", "tp"),
        P(None, "tp"),
        P(None, "tp"),
        P("tp", None),
    )
    body = functools.partial(shards, mesh.shape["sp"], mesh.shape["tp"])
    return jax.shard_map(
        body, mesh=mesh, in_specs=in_specs, out_specs=P(("sp", "tp"), None), check_vma=False
    )
```

time: 362 us -> 232 us (0.64)
  the two profiles are of different devices: /device:TPU:19 before, /device:TPU:27 now
where the time goes in v1:
time: 232 us
  Pallas kernels  230 us (99%)
    pallas_call x1, Pallas kernels, shards(): pl.pallas_call(functools.partial(layer, sp_count, tp_count), out_shape=ja...  230 us

profile of v1, /device:TPU:27, one launch (start us, length us, event | category | flops | bytes accessed | tf_op | source)
XLA Modules:
  0.0 231.9 jit_solution(14113772328753900900)
XLA Ops:
  0.0 230.3 %shard_map.145 = bf16[48,2048]{1,0:T(8,128)(2,1)} custom-call(bf16[192,128]{1,0:T(8,128)(2,1)} %q_a.1, bf16[192,128]{1,0:T(8,128)(2,1)} %k_a.1, bf16[192,128]{1,0:T(8,128)(2,1)} %q_b.1, bf16[192,128]{1,0:T(8,128)(2,1)} %k_b.1, bf16[192,256]{1,0:T(8,128)(2,1)} %vals.1, f32[2]{0:T(128)} %lambdas.1, f32[1,128]{1,0:T(1,128)} %bitcast.3, ...), custom_call_target="tpu_custom_call" | custom-call | tf_op jit(solution)/shard_map/pallas_call | solution.py:447
  230.3 1.6 copy.17

commit v2 on v1

--- a/solution.py
+++ b/solution.py
@@ -11,6 +11,7 @@
 far_below = -1e30
 halo = 16
 lanes = 2
+team = 2
 f32 = jnp.float32
 bf16 = jnp.bfloat16
 
@@ -39,6 +40,7 @@
     down_weight,
     out,
     kv,
+    w_own,
     w,
     down,
     out_w,
@@ -87,6 +89,15 @@
     w_rows = gate_weight.shape[0]
     ff = gate_weight.shape[1]
     taps = gate_taps.shape[0]
+    piece = w.shape[2]
+    shift = ff - piece
+    g = lax.rem(z, team)
+    partner = (z + 1 - 2 * g) * lanes + x
+    slot_rows = halo + rows
+
+    def columns(line):
+        return pl.multiple_of(lax.rem(line, team) * shift, 128)
+
 
     def remote(src, dst, send, recv, sp, tp):
         return pltpu.make_async_remote_copy(
@@ -111,14 +122,16 @@
         pltpu.make_async_copy(vals, kv.at[own, pl.ds(2 * key_width, value_width)], local.at[2]),
     )
     w_loads = (
-        pltpu.make_async_copy(gate_weight, w_block(0, s), local.at[3]),
-        pltpu.make_async_copy(up_weight, w_block(1, s), local.at[4]),
+        pltpu.make_async_copy(gate_weight, w_own.at[0], local.at[3]),
+        pltpu.make_async_copy(up_weight, w_own.at[1], local.at[4]),
+        pltpu.make_async_copy(gate_weight.at[:, pl.ds(columns(z), piece)], w_block(0, s), local.at[8]),
+        pltpu.make_async_copy(up_weight.at[:, pl.ds(columns(z), piece)], w_block(1, s), local.at[9]),
     )
     out_load = pltpu.make_async_copy(out_weight, out_w, local.at[5])
     res_load = pltpu.make_async_copy(
         residual.at[pl.ds(pl.multiple_of(t * part, 16), part)], res, local.at[6]
     )
-    down_load = pltpu.make_async_copy(down_weight, down, local.at[7])
+    down_load = pltpu.make_async_copy(down_weight.at[pl.ds(columns(z), piece)], down, local.at[7])
     for load in kv_loads + w_loads + (out_load, res_load, down_load):
         load.start()
 
@@ -142,7 +155,15 @@
             device_id_type=pl.DeviceIdType.MESH,
         )
 
-    pl.semaphore_wait(barrier, sp_count + tp_count - 2)
+    for i in range(1, tp_count):
+        pl.semaphore_signal(
+            barrier,
+            inc=1,
+            device_id=(partner, lax.rem(t + i, tp_count)),
+            device_id_type=pl.DeviceIdType.MESH,
+        )
+
+    pl.semaphore_wait(barrier, sp_count + 2 * tp_count - 3)
 
     def kvz(line, to, index):
         block = kv_block(line * lanes + x)
@@ -154,7 +175,8 @@
 
     def wz(c, line, to, index):
         block = w_block(c, line * lanes + x)
-        return remote(block, block, wz_send.at[c, index], wz_recv.at[c, line], to * lanes + x, t)
+        source = w_own.at[c, :, pl.ds(columns(to), piece)]
+        return remote(source, block, wz_send.at[c, index], wz_recv.at[c, line], to * lanes + x, t)
 
     def wx(c, line, lane):
         block = w_block(c, line * lanes + lane)
@@ -278,43 +300,66 @@
         ).wait_recv()
         stream[...] += part_in[source].astype(f32)
 
-    def ffn_rows(rank):
-        return pl.ds(pl.multiple_of(halo + rank * part, 16), part)
-
-    ffn[ffn_rows(t), :] = rms_scale(stream[...], mix_gain[...]).astype(bf16)
-
-    def gather_copy(i, rank):
+    def ffn_rows(slot, rank):
+        return pl.ds(pl.multiple_of(slot * slot_rows + halo + rank * part, 16), part)
+
+    ffn[ffn_rows(g, t), :] = rms_scale(stream[...], mix_gain[...]).astype(bf16)
+
+    def team_copy(slot):
+        rows_here = ffn.at[ffn_rows(slot, t)]
+        return remote(rows_here, rows_here, ag_send.at[slot, t], ag_recv.at[slot, t], partner, t)
+
+    def gather_copy(i, slot, rank):
         to = lax.rem(t + i, tp_count)
-        piece = ffn.at[ffn_rows(rank)]
-        return remote(piece, piece, ag_send.at[to], ag_recv.at[rank], s, to)
-
-    for i in range(1, tp_count):
-        gather_copy(i, t).start()
+        rows_here = ffn.at[ffn_rows(slot, rank)]
+        return remote(rows_here, rows_here, ag_send.at[slot, to], ag_recv.at[slot, rank], s, to)
+
+    team_copy(g).start()
+    for i in range(1, tp_count):
+        gather_copy(i, g, t).start()
     if early > 1:
         forward(2)
     for i in range(1, tp_count):
-        gather_copy(i, lax.rem(t + i, tp_count)).wait_recv()
-
-    halo_copy = remote(
-        ffn.at[pl.ds(rows, halo)],
-        ffn.at[pl.ds(0, halo)],
-        halo_send,
-        halo_recv,
-        lax.rem(s + 1, sp_count),
-        t,
-    )
+        gather_copy(i, g, lax.rem(t + i, tp_count)).wait_recv()
+
+    after = lax.rem(s + 1, sp_count)
+    after_line = after // lanes
+    after_slot = lax.rem(after_line, team)
+    after_other = (after_line + 1 - 2 * after_slot) * lanes + lax.rem(after, lanes)
+
+    def halo_copy(which, target, slot):
+        return remote(
+            ffn.at[pl.ds(pl.multiple_of(g * slot_rows + rows, 16), halo)],
+            ffn.at[pl.ds(pl.multiple_of(slot * slot_rows, 16), halo)],
+            halo_send.at[which],
+            halo_recv.at[slot],
+            target,
+            t,
+        )
 
     @pl.when(s < sp_count - 1)
     def _():
-        halo_copy.start()
-
-    @pl.when(s == 0)
-    def _():
-        ffn[0:halo, :] = jnp.zeros((halo, width), bf16)
-
-    @pl.when(s > 0)
-    def _():
-        halo_copy.wait_recv()
+        halo_copy(0, after, after_slot).start()
+
+        halo_copy(1, after_other, after_slot).start()
+
+    team_copy(1 - g).wait_recv()
+    for i in range(1, tp_count):
+        gather_copy(i, 1 - g, t).start()
+
+    for slot in range(team):
+        block = (z - g + slot) * lanes + x
+
+        @pl.when(block == 0)
+        def _():
+            ffn[slot * slot_rows : slot * slot_rows + halo, :] = jnp.zeros((halo, width), bf16)
+
+        @pl.when(block > 0)
+        def _():
+            halo_copy(0, mate, slot).wait_recv()
+
+    for i in range(1, tp_count):
+        gather_copy(i, 1 - g, lax.rem(t + i, tp_count)).wait_recv()
 
     acc[...] = jnp.zeros_like(acc)
 
@@ -355,47 +400,57 @@
         def _(i):
             project(i * 256, 256)
 
-    @pl.loop(0, ff // 128)
+    @pl.loop(0, piece // 128)
     def _(i):
         at = pl.ds(pl.multiple_of(i * 128, 128), 128)
-        made = []
-        for c, tap in enumerate((gate_taps, up_taps)):
-            total = None
-            for k in range(taps):
-                row = acc[c, pl.ds(halo - taps + 1 + k, rows), at].astype(bf16).astype(f32)
-                term = tap[pl.ds(k, 1), at] * row
-                total = term if total is None else total + term
-            made.append(total)
-        hidden[:, at] = (made[0] / (1 + jnp.exp(-made[0])) * made[1]).astype(bf16)
+        tap_at = pl.ds(pl.multiple_of(columns(z) + i * 128, 128), 128)
+        fresh = i * 128 >= g * (piece - shift)
+        for slot in range(team):
+            made = []
+            for c, tap in enumerate((gate_taps, up_taps)):
+                total = None
+                for k in range(taps):
+                    first = slot * slot_rows + halo - taps + 1 + k
+                    row = acc[c, pl.ds(first, rows), at].astype(bf16).astype(f32)
+                    term = tap[pl.ds(k, 1), tap_at] * row
+                    total = term if total is None else total + term
+                made.append(total)
+            value = made[0] / (1 + jnp.exp(-made[0])) * made[1]
+            hidden[slot * rows : (slot + 1) * rows, at] = jnp.where(fresh, value, 0.0).astype(bf16)
 
     down_load.wait()
     chunk = last_out.shape[3]
 
-    def last_copy(i, n, rank_to, rank_from):
+    def last_copy(n, far, rank, source, source_far):
         return remote(
-            last_out.at[rank_to, n],
-            last_in.at[rank_from, n],
-            last_send.at[rank_to, n],
-            last_recv.at[rank_from, n],
-            s,
-            lax.rem(t + i, tp_count),
+            last_out.at[far * tp_count + rank, n],
+            last_in.at[source_far * tp_count + source, n],
+            last_send.at[far * tp_count + rank, n],
+            last_recv.at[source_far * tp_count + source, n],
+            partner if far else s,
+            rank,
         )
 
     for n in range(width // chunk):
-        product = jnp.dot(
-            hidden[...], down[:, n * chunk : (n + 1) * chunk], preferred_element_type=f32
-        ).astype(bf16)
-        for r in range(tp_count):
-            last_out[r, n] = product[r * part : (r + 1) * part]
-        for i in range(1, tp_count):
-            last_copy(i, n, lax.rem(t + i, tp_count), t).start()
+        for far in (1, 0):
+            slot = 1 - g if far else g
+            product = jnp.dot(
+                hidden[pl.ds(pl.multiple_of(slot * rows, 16), rows), :],
+                down[:, n * chunk : (n + 1) * chunk],
+                preferred_element_type=f32,
+            ).astype(bf16)
+            for r in range(tp_count):
+                last_out[far * tp_count + r, n] = product[r * part : (r + 1) * part]
+            for i in range(1 - far, tp_count):
+                last_copy(n, far, lax.rem(t + i, tp_count), t, far).start()
     for n in range(width // chunk):
         at = slice(n * chunk, (n + 1) * chunk)
         total = stream[:, at] + last_out[t, n].astype(f32)
-        for i in range(1, tp_count):
-            source = lax.rem(t + i, tp_count)
-            last_copy(i, n, source, source).wait_recv()
-            total = total + last_in[source, n].astype(f32)
+        for far in (0, 1):
+            for i in range(1 - far, tp_count):
+                source = lax.rem(t + i, tp_count)
+                last_copy(n, far, source, source, far).wait_recv()
+                total = total + last_in[far * tp_count + source, n].astype(f32)
         out[:, at] = total.astype(bf16)
 
     @pl.loop(z + 1, lines)
@@ -417,15 +472,21 @@
         for c in range(2):
             wx(c, line, x).wait_send()
 
+    team_copy(g).wait_send()
     for i in range(1, tp_count):
         part_copy(i).wait_send()
-        gather_copy(i, t).wait_send()
-        for n in range(width // chunk):
-            last_copy(i, n, lax.rem(t + i, tp_count), t).wait_send()
+        for slot in range(team):
+            gather_copy(i, slot, t).wait_send()
+    for n in range(width // chunk):
+        for far in (0, 1):
+            for i in range(1 - far, tp_count):
+                last_copy(n, far, lax.rem(t + i, tp_count), t, far).wait_send()
 
     @pl.when(s < sp_count - 1)
     def _():
-        halo_copy.wait_send()
+        halo_copy(0, after, after_slot).wait_send()
+
+        halo_copy(1, after_other, after_slot).wait_send()
 
 
 def shards(sp_count, tp_count, *args):
@@ -436,6 +497,7 @@
     part = rows // tp_count
     lines = sp_count // lanes
     chunk = 512 if width % 512 == 0 else width
+    piece = -(-ff // (team * 128)) * 128
     args = list(args)
     args[6] = head_gain.reshape(1, -1)
     args[9] = mix_gain.reshape(1, -1)
@@ -451,20 +513,21 @@
         out_specs=vmem,
         scratch_shapes=[
             pltpu.VMEM((sp_count * rows, 2 * q_a.shape[1] + vals.shape[1]), bf16),
-            pltpu.VMEM((2, sp_count * w_rows, ff), bf16),
-            pltpu.VMEM(down.shape, bf16),
+            pltpu.VMEM((2, w_rows, ff), bf16),
+            pltpu.VMEM((2, sp_count * w_rows, piece), bf16),
+            pltpu.VMEM((piece, width), bf16),
             pltpu.VMEM(out_weight.shape, bf16),
             pltpu.VMEM((part, width), bf16),
             pltpu.VMEM((rows, vals.shape[1]), bf16),
             pltpu.VMEM((tp_count, part, width), bf16),
             pltpu.VMEM((tp_count, part, width), bf16),
             pltpu.VMEM((part, width), f32),
-            pltpu.VMEM((halo + rows, width), bf16),
-            pltpu.VMEM((2, halo + rows, ff), f32),
-            pltpu.VMEM((rows, ff), bf16),
-            pltpu.VMEM((tp_count, width // chunk, part, chunk), bf16),
-            pltpu.VMEM((tp_count, width // chunk, part, chunk), bf16),
-            dma((8,)),
+            pltpu.VMEM((team * (halo + rows), width), bf16),
+            pltpu.VMEM((2, team * (halo + rows), piece), f32),
+            pltpu.VMEM((team * rows, piece), bf16),
+            pltpu.VMEM((team * tp_count, width // chunk, part, chunk), bf16),
+            pltpu.VMEM((team * tp_count, width // chunk, part, chunk), bf16),
+            dma((10,)),
             dma((lines,)),
             dma((lines,)),
             dma((lines,)),
@@ -475,12 +538,12 @@
             dma((2, lines)),
             dma((tp_count,)),
             dma((tp_count,)),
-            dma((tp_count,)),
-            dma((tp_count,)),
-            dma(()),
-            dma(()),
-            dma((tp_count, width // chunk)),
-            dma((tp_count, width // chunk)),
+            dma((team, tp_count)),
+            dma((team, tp_count)),
+            dma((2,)),
+            dma((team,)),
+            dma((team * tp_count, width // chunk)),
+            dma((team * tp_count, width // chunk)),
         ],
         compiler_params=pltpu.CompilerParams(
             collective_id=0, has_side_effects=True, vmem_limit_bytes=60 * 1024 * 1024

time: 232 us -> 159 us (0.69)
  the two profiles are of different devices: /device:TPU:27 before, /device:TPU:19 now
where the time goes in v2:
time: 159 us
  Pallas kernels  157 us (99%)
  local copies, waits for them, and re-layouts  1.62 us (1%)
    pallas_call x1, Pallas kernels, shards(): pl.pallas_call(functools.partial(layer, sp_count, tp_count), out_shape=ja...  157 us

profile of v2, /device:TPU:19, one launch (start us, length us, event | category | flops | bytes accessed | tf_op | source)
XLA Modules:
  0.0 158.8 jit_solution(6792003278578425213)
XLA Ops:
  0.0 157.2 %shard_map.145 = bf16[48,2048]{1,0:T(8,128)(2,1)} custom-call(bf16[192,128]{1,0:T(8,128)(2,1)} %q_a.1, bf16[192,128]{1,0:T(8,128)(2,1)} %k_a.1, bf16[192,128]{1,0:T(8,128)(2,1)} %q_b.1, bf16[192,128]{1,0:T(8,128)(2,1)} %k_b.1, bf16[192,256]{1,0:T(8,128)(2,1)} %vals.1, f32[2]{0:T(128)} %lambdas.1, f32[1,128]{1,0:T(1,128)} %bitcast.3, ...), custom_call_target="tpu_custom_call" | custom-call | tf_op jit(solution)/shard_map/pallas_call | solution.py:509
  157.2 1.6 %copy.17 = bf16[48,2048]{1,0:T(8,128)(2,1)} copy(bf16[48,2048]{1,0:T(8,128)(2,1)} %shard_map.145) | data formatting | bytes 393216

commit v3 on v2

--- a/solution.py
+++ b/solution.py
@@ -52,6 +52,8 @@
     ffn,
     acc,
     hidden,
+    pair_out,
+    pair_in,
     last_out,
     last_in,
     local,
@@ -69,6 +71,8 @@
     ag_recv,
     halo_send,
     halo_recv,
+    pair_send,
+    pair_recv,
     last_send,
     last_recv,
 ):
@@ -193,11 +197,14 @@
     for load in w_loads:
         load.wait()
 
-    @pl.loop(1, lines)
-    def _(i):
+    def send_weights(i):
         to = lax.rem(z + lines - i, lines)
         for c in range(2):
             wz(c, z, to, to).start()
+
+    @pl.loop(1, lines - 1)
+    def _(i):
+        send_weights(i)
 
     @pl.loop(0, z)
     def _(i):
@@ -269,7 +276,7 @@
             wz(c, line, mate // lanes, line).wait_recv()
             wx(c, line, x).start()
 
-    early = min(2, lines - 1)
+    early = min(3, lines - 1)
     if early > 0:
         forward(1)
 
@@ -315,6 +322,7 @@
         return remote(rows_here, rows_here, ag_send.at[slot, to], ag_recv.at[slot, rank], s, to)
 
     team_copy(g).start()
+    send_weights(lines - 1)
     for i in range(1, tp_count):
         gather_copy(i, g, t).start()
     if early > 1:
@@ -346,6 +354,8 @@
     team_copy(1 - g).wait_recv()
     for i in range(1, tp_count):
         gather_copy(i, 1 - g, t).start()
+    if early > 2:
+        forward(3)
 
     for slot in range(team):
         block = (z - g + slot) * lanes + x
@@ -419,38 +429,63 @@
             hidden[slot * rows : (slot + 1) * rows, at] = jnp.where(fresh, value, 0.0).astype(bf16)
 
     down_load.wait()
-    chunk = last_out.shape[3]
-
-    def last_copy(n, far, rank, source, source_far):
+    chunk = last_out.shape[2]
+    chunks = width // chunk
+    pairs = tp_count // 2
+    c_own = lax.rem(t, 2)
+    k_own = t // 2
+
+    def pair_rows(far, k):
+        return pl.ds(pl.multiple_of((far * pairs + k) * part, 16), part)
+
+    def pair_copy(n):
         return remote(
-            last_out.at[far * tp_count + rank, n],
-            last_in.at[source_far * tp_count + source, n],
-            last_send.at[far * tp_count + rank, n],
-            last_recv.at[source_far * tp_count + source, n],
+            pair_out.at[n, 1 - c_own],
+            pair_in.at[n],
+            pair_send.at[n],
+            pair_recv.at[n],
+            s,
+            t + 1 - 2 * c_own,
+        )
+
+    def last_copy(n, far, k, source):
+        return remote(
+            last_out.at[n, pair_rows(far, k)],
+            last_in.at[n, pair_rows(far, source)],
+            last_send.at[n, far * pairs + k],
+            last_recv.at[n, far * pairs + source],
             partner if far else s,
-            rank,
-        )
-
-    for n in range(width // chunk):
-        for far in (1, 0):
-            slot = 1 - g if far else g
-            product = jnp.dot(
-                hidden[pl.ds(pl.multiple_of(slot * rows, 16), rows), :],
-                down[:, n * chunk : (n + 1) * chunk],
-                preferred_element_type=f32,
-            ).astype(bf16)
-            for r in range(tp_count):
-                last_out[far * tp_count + r, n] = product[r * part : (r + 1) * part]
-            for i in range(1 - far, tp_count):
-                last_copy(n, far, lax.rem(t + i, tp_count), t, far).start()
-    for n in range(width // chunk):
+            2 * k + c_own,
+        )
+
+    for n in range(chunks + 1):
+        if n < chunks:
+            for far in (1, 0):
+                slot = 1 - g if far else g
+                product = jnp.dot(
+                    hidden[pl.ds(pl.multiple_of(slot * rows, 16), rows), :],
+                    down[:, n * chunk : (n + 1) * chunk],
+                    preferred_element_type=f32,
+                ).astype(bf16)
+                for r in range(tp_count):
+                    first = (far * pairs + r // 2) * part
+                    pair_out[n, r % 2, first : first + part] = product[r * part : (r + 1) * part]
+            pair_copy(n).start()
+        if n > 0:
+            pair_copy(n - 1).wait_recv()
+            both = pair_out[n - 1, c_own].astype(f32) + pair_in[n - 1].astype(f32)
+            last_out[n - 1] = both.astype(bf16)
+            for far in (1, 0):
+                for i in range(1 - far, pairs):
+                    last_copy(n - 1, far, lax.rem(k_own + i, pairs), k_own).start()
+    for n in range(chunks):
         at = slice(n * chunk, (n + 1) * chunk)
-        total = stream[:, at] + last_out[t, n].astype(f32)
+        total = stream[:, at] + last_out[n, pair_rows(0, k_own), :].astype(f32)
         for far in (0, 1):
-            for i in range(1 - far, tp_count):
-                source = lax.rem(t + i, tp_count)
-                last_copy(n, far, source, source, far).wait_recv()
-                total = total + last_in[far * tp_count + source, n].astype(f32)
+            for i in range(1 - far, pairs):
+                source = lax.rem(k_own + i, pairs)
+                last_copy(n, far, source, source).wait_recv()
+                total = total + last_in[n, pair_rows(far, source), :].astype(f32)
         out[:, at] = total.astype(bf16)
 
     @pl.loop(z + 1, lines)
@@ -477,10 +512,11 @@
         part_copy(i).wait_send()
         for slot in range(team):
             gather_copy(i, slot, t).wait_send()
-    for n in range(width // chunk):
+    for n in range(chunks):
+        pair_copy(n).wait_send()
         for far in (0, 1):
-            for i in range(1 - far, tp_count):
-                last_copy(n, far, lax.rem(t + i, tp_count), t, far).wait_send()
+            for i in range(1 - far, pairs):
+                last_copy(n, far, lax.rem(k_own + i, pairs), k_own).wait_send()
 
     @pl.when(s < sp_count - 1)
     def _():
@@ -497,6 +533,7 @@
     part = rows // tp_count
     lines = sp_count // lanes
     chunk = 512 if width % 512 == 0 else width
+    share = team * tp_count // 2 * part
     piece = -(-ff // (team * 128)) * 128
     args = list(args)
     args[6] = head_gain.reshape(1, -1)
@@ -525,8 +562,10 @@
             pltpu.VMEM((team * (halo + rows), width), bf16),
             pltpu.VMEM((2, team * (halo + rows), piece), f32),
             pltpu.VMEM((team * rows, piece), bf16),
-            pltpu.VMEM((team * tp_count, width // chunk, part, chunk), bf16),
-            pltpu.VMEM((team * tp_count, width // chunk, part, chunk), bf16),
+            pltpu.VMEM((width // chunk, 2, share, chunk), bf16),
+            pltpu.VMEM((width // chunk, share, chunk), bf16),
+            pltpu.VMEM((width // chunk, share, chunk), bf16),
+            pltpu.VMEM((width // chunk, share, chunk), bf16),
             dma((10,)),
             dma((lines,)),
             dma((lines,)),
@@ -542,8 +581,10 @@
             dma((team, tp_count)),
             dma((2,)),
             dma((team,)),
-            dma((team * tp_count, width // chunk)),
-            dma((team * tp_count, width // chunk)),
+            dma((width // chunk,)),
+            dma((width // chunk,)),
+            dma((width // chunk, team * tp_count // 2)),
+            dma((width // chunk, team * tp_count // 2)),
         ],
         compiler_params=pltpu.CompilerParams(
             collective_id=0, has_side_effects=True, vmem_limit_bytes=60 * 1024 * 1024

time: 159 us -> 155 us (0.975)
  Pallas kernels: 157 us -> 153 us
    pallas_call x1, Pallas kernels: 157 us -> 153 us  [shards(): pl.pallas_call(functools.partial(layer, sp_count, tp_count), out_shape=ja...]
where the time goes in v3:
time: 155 us; the launch traced here: 154 us
  Pallas kernels  153 us (99%)
  local copies, waits for them, and re-layouts  1.62 us (1%)
    pallas_call x1, Pallas kernels, shards(): pl.pallas_call(functools.partial(layer, sp_count, tp_count), out_shape=ja...  153 us

profile of v3, /device:TPU:19, one launch (start us, length us, event | category | flops | bytes accessed | tf_op | source)
XLA Modules:
  0.0 154.3 jit_solution(17463026762482345658)
XLA Ops:
  0.0 152.7 %shard_map.145 = bf16[48,2048]{1,0:T(8,128)(2,1)} custom-call(bf16[192,128]{1,0:T(8,128)(2,1)} %q_a.1, bf16[192,128]{1,0:T(8,128)(2,1)} %k_a.1, bf16[192,128]{1,0:T(8,128)(2,1)} %q_b.1, bf16[192,128]{1,0:T(8,128)(2,1)} %k_b.1, bf16[192,256]{1,0:T(8,128)(2,1)} %vals.1, f32[2]{0:T(128)} %lambdas.1, f32[1,128]{1,0:T(1,128)} %bitcast.3, ...), custom_call_target="tpu_custom_call" | custom-call | tf_op jit(solution)/shard_map/pallas_call | solution.py:546
  152.7 1.6 %copy.17 = bf16[48,2048]{1,0:T(8,128)(2,1)} copy(bf16[48,2048]{1,0:T(8,128)(2,1)} %shard_map.145) | data formatting | bytes 393216
